TPU v7x, 32 devices: a whole 2x2x4 slice. The times are simulated.
32 devices in a mesh: grp: 2 (over y), sp: 4 (over z), tp: 4 (over x, core).
Axes of the slice: x: 2, y: 2, z: 4, core: 2. Of those that a mesh axis runs over, the one named last changes fastest.
Arguments:
- hidden_in: bfloat16 [3072, 4096], P(('grp', 'sp'), 'tp'), parts along dimension 0, may hold values from -30 to 30
- in_gain: float32 [2, 4096], P(None, 'tp'), may hold values from 0.1 to 1.9
- w_value: bfloat16 [2, 4096, 2048], P(None, 'sp', 'tp'), may hold values from -0.09375 to 0.09375
- w_gate: bfloat16 [2, 4096, 2048], P(None, 'sp', 'tp'), may hold values from -0.09375 to 0.09375
- conv_taps: float32 [2, 31, 2048], P(None, None, 'tp'), may hold values from -9 to 9
- norm_gain: float32 [2, 2048], P(None, 'tp'), may hold values from 0.1 to 1.9
- norm_shift: float32 [2, 2048], P(None, 'tp'), may hold values from -3 to 3
- w_out: bfloat16 [2, 2048, 4096], P(None, 'tp', 'sp'), may hold values from -0.125 to 0.125
Outputs:
- hidden_out: bfloat16 [3072, 4096], P(('grp', 'sp'), 'tp'), parts along dimension 0
There are 2 independent parts, one for each index of `grp`. A program takes and returns all parts, laid end to end along the dimension named above; an argument that names none is the same for every part. Nothing has to cross between parts.
All inputs are finite; a program needn't handle non-finite values.
Results may differ from a plain program's by a relative error of at most 0.013.
Values may be sent and summed in bfloat16 or wider, within the bound.
A program may use at most 64 MiB of HBM per device.

v0:
```python
import jax
import jax.numpy as jnp
from jax import lax
from jax.sharding import PartitionSpec as P

D = 4096
C = 2048
epsilon = 1e-06


def passed_along(value, axis, steps):
    count = lax.axis_size(axis)
    initial, last = (max(0, -steps), min(count, count - steps))
    return lax.ppermute(value, axis, [(source, source + steps) for source in range(initial, last)])


def depthwise(extended, kernel_taps):
    conved = lax.conv_general_dilated(
        extended.astype(jnp.float32)[None],
        kernel_taps[:, None, :],
        (1,),
        [(0, 0)],
        dimension_numbers=("NWC", "WIO", "NWC"),
        feature_group_count=extended.shape[1],
        precision=lax.Precision.HIGHEST,
    )
    return conved[0]


def shards(hidden_in, in_gain, w_value, w_gate, conv_taps, norm_gain, norm_shift, w_out):
    layer_count = w_value.shape[0]
    reach_rows = conv_taps.shape[1] - 1
    value_all, gate_all = (
        lax.all_gather(w_value, "sp", axis=1, tiled=True),
        lax.all_gather(w_gate, "sp", axis=1, tiled=True),
    )
    out_all = lax.all_gather(w_out, "sp", axis=2, tiled=True)
    current = hidden_in
    for layer_idx in range(layer_count):
        widened = current.astype(jnp.float32)
        squares = lax.psum(jnp.sum(widened * widened, axis=1), "tp")
        normalized = (
            widened * lax.rsqrt(squares / D + epsilon)[:, None] * in_gain[layer_idx]
        ).astype(jnp.bfloat16)
        gathered = lax.all_gather(normalized, "tp", axis=1, tiled=True)
        value_part = jnp.dot(gathered, value_all[layer_idx], preferred_element_type=jnp.float32)
        gate_part = jnp.dot(gathered, gate_all[layer_idx], preferred_element_type=jnp.float32)
        gated = (value_part * jax.nn.sigmoid(gate_part)).astype(jnp.bfloat16)
        before = passed_along(gated[gated.shape[0] - reach_rows :], "sp", 1)
        extended = jnp.concatenate([before, gated], axis=0)
        residual = current
        conved = depthwise(extended, conv_taps[layer_idx])
        total_sum, total_squares = lax.psum(
            (jnp.sum(conved, axis=1), jnp.sum(conved * conved, axis=1)), "tp"
        )
        row_mean = total_sum / C
        spread = total_squares / C - row_mean * row_mean
        normed = (conved - row_mean[:, None]) * lax.rsqrt(spread + epsilon)[:, None] * norm_gain[
            layer_idx
        ] + norm_shift[layer_idx]
        mixed_out = jax.nn.silu(normed).astype(jnp.bfloat16)
        partial_value = jnp.dot(mixed_out, out_all[layer_idx], preferred_element_type=jnp.float32)
        summed = lax.psum_scatter(
            partial_value.astype(jnp.bfloat16), "tp", scatter_dimension=1, tiled=True
        ).astype(jnp.float32)
        current = (residual.astype(jnp.float32) + summed).astype(jnp.bfloat16)
    return current


def solution(mesh):
    placed = (
        P(("grp", "sp"), "tp"),
        P(None, "tp"),
        P(None, "sp", "tp"),
        P(None, "sp", "tp"),
        P(None, None, "tp"),
        P(None, "tp"),
        P(None, "tp"),
        P(None, "tp", "sp"),
    )
    return jax.shard_map(
        shards, mesh=mesh, in_specs=placed, out_specs=P(("grp", "sp"), "tp"), check_vma=False
    )
```

profile of v0, /device:TPU:0, one launch (start us, length us, event | category | flops | bytes accessed | tf_op | source)
XLA Modules:
  0.0 657.1 jit_solution(9422213232833642842)
XLA Ops:
  6.5 1.4 fusion.4
  7.9 8.4 %psum.42 = f32[384]{0:T(512)S(1)} all-reduce(f32[384]{0:T(512)S(1)} %fusion.4), channel_id=1, replica_groups=mesh['grp'=2,'sp'=4,'tp'=4] {'tp'}, use_global_device_ids=true, to_apply=%region_1.0 | all-reduce | flops 384 | bytes 3072 | tf_op jit(solution)/shard_map/psum | solution.py:41
  16.3 0.8 fusion.62
  17.1 2.3 fusion.6
  19.4 0.7 all-gather.10.cloned.1.call-update
  20.2 0.7 all-gather.8.cloned.1.call-update
  20.9 0.5 all-gather.12.cloned.1.call-update
  21.5 26.8 %all-gather.6.cloned.1.call-done = bf16[384,4096]{1,0:T(8,128)(2,1)} async-done(((bf16[384,1024]{1,0:T(8,128)(2,1)}), bf16[384,4096]{1,0:T(8,128)(2,1)}) %all-gather.6.cloned.1.call-update) | async-done | bytes 3145744 | tf_op jit(solution)/shard_map/all_gather | solution.py:45
  48.3 151.2 %all-gather.10.cloned.1.call-done = bf16[2,4096,512]{2,1,0:T(8,128)(2,1)} async-done(((bf16[2,1024,512]{2,1,0:T(8,128)(2,1)}), bf16[2,4096,512]{2,1,0:T(8,128)(2,1)}) %all-gather.10.cloned.1.call-update) | async-done | bytes 8388624 | tf_op jit(solution)/shard_map/all_gather | solution.py:35
  199.5 5.9 fusion.23
  205.5 143.5 %all-gather.8.cloned.1.call-done = bf16[2,4096,512]{2,1,0:T(8,128)(2,1)} async-done(((bf16[2,1024,512]{2,1,0:T(8,128)(2,1)}), bf16[2,4096,512]{2,1,0:T(8,128)(2,1)}) %all-gather.8.cloned.1.call-update) | async-done | bytes 8388624 | tf_op jit(solution)/shard_map/all_gather | solution.py:34
  349.0 4.2 fusion.25
  353.2 1.4 collective-permute-start
  354.6 1.6 collective-permute-done
  356.6 1.9 fusion.65
  359.9 6.6 all-reduce.1
  366.5 131.7 %all-gather.12.cloned.1.call-done = bf16[2,512,4096]{2,1,0:T(8,128)(2,1)} async-done(((bf16[2,512,1024]{2,1,0:T(8,128)(2,1)}), bf16[2,512,4096]{2,1,0:T(8,128)(2,1)}) %all-gather.12.cloned.1.call-update) | async-done | bytes 8388624 | tf_op jit(solution)/shard_map/all_gather | solution.py:37
  498.2 5.9 convolution_convert_fusion.1
  504.2 36.0 %reduce-scatter.3.cloned.1.call-done = bf16[384,1024]{1,0:T(8,128)(2,1)} async-done(((bf16[384,4096]{1,0:T(8,128)(2,1)}), bf16[384,1024]{1,0:T(8,128)(2,1)}) %reduce-scatter.3.cloned.1.call-update) | async-done | bytes 786448 | tf_op jit(solution)/shard_map/reduce_scatter | solution.py:63
  540.2 1.5 fusion.8
  541.6 5.8 psum.45
  547.4 2.3 fusion.10
  550.0 29.1 %all-gather.14.cloned.1.call-done = bf16[384,4096]{1,0:T(8,128)(2,1)} async-done(((bf16[384,1024]{1,0:T(8,128)(2,1)}), bf16[384,4096]{1,0:T(8,128)(2,1)}) %all-gather.14.cloned.1.call-update) | async-done | bytes 3145744 | tf_op jit(solution)/shard_map/all_gather | solution.py:45
  579.0 5.2 fusion.21
  584.2 4.0 fusion.24
  588.3 3.4 collective-permute-start.1
  591.7 1.6 collective-permute-done.1
  593.7 2.0 fusion.66
  597.2 5.9 all-reduce
  603.2 5.9 convolution_convert_fusion
  609.1 38.7 %reduce-scatter.5.cloned.1.call-done = bf16[384,1024]{1,0:T(8,128)(2,1)} async-done(((bf16[384,4096]{1,0:T(8,128)(2,1)}), bf16[384,1024]{1,0:T(8,128)(2,1)}) %reduce-scatter.5.cloned.1.call-update) | async-done | bytes 786448 | tf_op jit(solution)/shard_map/reduce_scatter | solution.py:63
  647.8 2.4 fusion.11
  (56 shorter events, 4.2 us)
Async XLA Ops:
  6.5 41.8 %all-gather.6.cloned.1.call-start = ((), (), s32[]{:S(2)}) async-start(), calls=%async_computation.2 | async-start | bytes 3932160 | tf_op jit(solution)/shard_map/all_gather | solution.py:45
  19.4 2.1 copy-start.2
  19.4 180.2 %all-gather.10.cloned.1.call-start = ((), (), s32[]{:S(2)}) async-start(), calls=%async_computation.4 | async-start | bytes 10485760 | tf_op jit(solution)/shard_map/all_gather | solution.py:35
  20.1 328.8 %all-gather.8.cloned.1.call-start = ((), (), s32[]{:S(2)}) async-start(), calls=%async_computation.3 | async-start | bytes 10485760 | tf_op jit(solution)/shard_map/all_gather | solution.py:34
  20.9 477.4 %all-gather.12.cloned.1.call-start = ((), (), s32[]{:S(2)}) async-start(), calls=%async_computation.5 | async-start | bytes 10485760 | tf_op jit(solution)/shard_map/all_gather | solution.py:37
  21.4 518.8 %reduce-scatter.3.cloned.1.call-start = ((), (), s32[]{:S(2)}) async-start(), calls=%async_computation.6 | async-start | bytes 3932160 | tf_op jit(solution)/shard_map/reduce_scatter | solution.py:63
  48.3 300.6 %copy-start.4 = (bf16[384,4096]{1,0:T(8,128)(2,1)S(1)}, bf16[384,4096]{1,0:T(8,128)(2,1)}, u32[]{:S(2)}) copy-start(bf16[384,4096]{1,0:T(8,128)(2,1)} %all-gather.6.cloned.1.call-done) | copy-start | bytes 9437188
  205.5 149.1 %copy-start.3 = (f32[2,512]{1,0:T(2,128)S(1)}, f32[2,512]{1,0:T(2,128)}, u32[]{:S(2)}) copy-start(f32[2,512]{1,0:T(2,128)} %param.14) | copy-start | bytes 12292
  353.1 3.5 copy-start.6
  353.2 3.5 copy-start.7
  353.2 3.0 collective-permute-start
  504.1 36.1 %copy-start = (bf16[384,1024]{1,0:T(8,128)(2,1)S(1)}, bf16[384,1024]{1,0:T(8,128)(2,1)}, u32[]{:S(2)}) copy-start(bf16[384,1024]{1,0:T(8,128)(2,1)} %param.8) | copy-start | bytes 2359300
  504.1 74.9 %all-gather.14.cloned.1.call-start = ((), (), s32[]{:S(2)}) async-start(), calls=%async_computation.7 | async-start | bytes 3932160 | tf_op jit(solution)/shard_map/all_gather | solution.py:45
  549.8 98.0 %reduce-scatter.5.cloned.1.call-start = ((), (), s32[]{:S(2)}) async-start(), calls=%async_computation.8 | async-start | bytes 3932160 | tf_op jit(solution)/shard_map/reduce_scatter | solution.py:63
  579.0 5.2 copy-start.5
  588.3 5.0 collective-permute-start.1
  609.1 38.7 %copy-start.1 = (bf16[384,1024]{1,0:T(8,128)(2,1)S(1)}, bf16[384,1024]{1,0:T(8,128)(2,1)}, u32[]{:S(2)}) copy-start(bf16[384,1024]{1,0:T(8,128)(2,1)} %reduce-scatter.3.cloned.1.call-done) | copy-start | bytes 2359300
Sparse Core Ops, SparseCore 0:
  19.5 28.8 all-gather.5
  49.9 149.6 all-gather.9
  201.1 147.7 all-gather.7
  350.4 147.7 all-gather.11
  504.2 35.8 reduce-scatter.2
  549.9 29.1 all-gather.13
  609.2 38.5 reduce-scatter.4
where the time goes:
time: 658 us; the launch traced here: 657 us
  waiting for transfers between devices  562 us (85%)
  matrix products  35 us (5%)
  blocking collectives  26.6 us (4%)
  between operations  13.8 us (2%)
  other arithmetic  10.6 us (2%)
    all_gather x1, waiting for transfers between devices, shards(): lax.all_gather(w_gate, 'sp', axis=1, tiled=True)  151 us
    all_gather x1, waiting for transfers between devices, shards(): lax.all_gather(w_value, 'sp', axis=1, tiled=True)  143 us
    all_gather x1, waiting for transfers between devices, shards(): out_all = lax.all_gather(w_out, 'sp', axis=2, tiled=True)  132 us
    reduce_scatter x2, waiting for transfers between devices, shards(): lax.psum_scatter(partial_value.astype(jnp.bfloat16), 'tp', scatter_dimens...  74.7 us
    all_gather x2, waiting for transfers between devices, shards(): gathered = lax.all_gather(normalized, 'tp', axis=1, tiled=True)  55.9 us
    psum x2, blocking collectives, shards(): squares = lax.psum(jnp.sum(widened * widened, axis=1), 'tp')  14.1 us
  transfers between devices with their start and end apart: 9, of which 9 were waited for; matrix products, arithmetic and copies ran while one was open for 2% of the time, Pallas kernels for 0%

commit v1 on v0

--- a/solution.py
+++ b/solution.py
@@ -42,7 +42,14 @@
         normalized = (
             widened * lax.rsqrt(squares / D + epsilon)[:, None] * in_gain[layer_idx]
         ).astype(jnp.bfloat16)
-        gathered = lax.all_gather(normalized, "tp", axis=1, tiled=True)
+        ring = [normalized]
+        for hop in range(3):
+            ring.append(lax.ppermute(ring[-1], "tp", [(dev, (dev + 1) % 4) for dev in range(4)]))
+        gathered = jnp.roll(
+            jnp.concatenate(ring[::-1], axis=1),
+            (lax.axis_index("tp") + 1) * ring[0].shape[1],
+            axis=1,
+        )
         value_part = jnp.dot(gathered, value_all[layer_idx], preferred_element_type=jnp.float32)
         gate_part = jnp.dot(gathered, gate_all[layer_idx], preferred_element_type=jnp.float32)
         gated = (value_part * jax.nn.sigmoid(gate_part)).astype(jnp.bfloat16)

time: 658 us -> 626 us (0.951)
  waiting for transfers between devices: 562 us -> 526 us
  other arithmetic: 10.6 us -> 19.1 us
    ppermute x0 -> x6, waiting for transfers between devices: none -> 68.5 us  [shards(): lax.ppermute(ring[-1], 'tp', [(dev, (dev + 1) % 4) for dev in range(4)])]
    all_gather x2 -> x0, waiting for transfers between devices: 55.9 us -> none  [shards(): gathered = lax.all_gather(normalized, 'tp', axis=1, tiled=True)]
    all_gather x1, waiting for transfers between devices: 151 us -> 102 us  [shards(): lax.all_gather(w_gate, 'sp', axis=1, tiled=True)]
    concatenate x0 -> x2, other arithmetic: none -> 12.6 us  [shards(): jnp.roll(jnp.concatenate(ring[::-1], axis=1), (lax.axis_index('tp') + 1)...]
  transfers between devices with their start and end apart: 9 -> 13, of which waited for: 9 -> 13; matrix products, arithmetic and copies ran while one was open for 2% -> 3% of each run, Pallas kernels for 0% -> 0%
where the time goes in v1:
time: 626 us; the launch traced here: 625 us
  waiting for transfers between devices  526 us (84%)
  matrix products  31.8 us (5%)
  blocking collectives  26.3 us (4%)
  other arithmetic  19.1 us (3%)
  between operations  13.5 us (2%)
    all_gather x1, waiting for transfers between devices, shards(): lax.all_gather(w_value, 'sp', axis=1, tiled=True)  144 us
    all_gather x1, waiting for transfers between devices, shards(): out_all = lax.all_gather(w_out, 'sp', axis=2, tiled=True)  131 us
    all_gather x1, waiting for transfers between devices, shards(): lax.all_gather(w_gate, 'sp', axis=1, tiled=True)  102 us
    reduce_scatter x2, waiting for transfers between devices, shards(): lax.psum_scatter(partial_value.astype(jnp.bfloat16), 'tp', scatter_dimens...  75 us
    ppermute x6, waiting for transfers between devices, shards(): lax.ppermute(ring[-1], 'tp', [(dev, (dev + 1) % 4) for dev in range(4)])  68.5 us
    psum x2, blocking collectives, shards(): squares = lax.psum(jnp.sum(widened * widened, axis=1), 'tp')  14.1 us
    concatenate x2, other arithmetic, shards(): jnp.roll(jnp.concatenate(ring[::-1], axis=1), (lax.axis_index('tp') + 1)...  12.6 us
  transfers between devices with their start and end apart: 13, of which 13 were waited for; matrix products, arithmetic and copies ran while one was open for 3% of the time, Pallas kernels for 0%

profile of v1, /device:TPU:0, one launch (start us, length us, event | category | flops | bytes accessed | tf_op | source)
XLA Modules:
  0.0 625.5 jit_solution(3969366722602050028)
XLA Ops:
  9.0 8.4 %psum.42 = f32[384]{0:T(512)S(1)} all-reduce(f32[384]{0:T(512)S(1)} %fusion.18), channel_id=1, replica_groups=mesh['grp'=2,'sp'=4,'tp'=4] {'tp'}, use_global_device_ids=true, to_apply=%region_1.0 | all-reduce | flops 384 | bytes 3072 | tf_op jit(solution)/shard_map/psum | solution.py:41
  17.7 11.4 %collective-permute-done = bf16[384,1024]{1,0:T(8,128)(2,1)S(1)} collective-permute-done((bf16[384,1024]{1,0:T(8,128)(2,1)S(1)}, bf16[384,1024]{1,0:T(8,128)(2,1)S(1)}, u32[]{:S(2)}, u32[]{:S(2)}) %collective-permute-start) | collective-permute-done | bytes 786464 | tf_op jit(solution)/shard_map/ppermute | solution.py:47
  29.1 11.4 %collective-permute-done.1 = bf16[384,1024]{1,0:T(8,128)(2,1)S(1)} collective-permute-done((bf16[384,1024]{1,0:T(8,128)(2,1)S(1)}, bf16[384,1024]{1,0:T(8,128)(2,1)S(1)}, u32[]{:S(2)}, u32[]{:S(2)}) %collective-permute-start.1) | collective-permute-done | bytes 786464 | tf_op jit(solution)/shard_map/ppermute | solution.py:47
  40.6 11.5 %collective-permute-done.2 = bf16[384,1024]{1,0:T(8,128)(2,1)} collective-permute-done((bf16[384,1024]{1,0:T(8,128)(2,1)S(1)}, bf16[384,1024]{1,0:T(8,128)(2,1)}, u32[]{:S(2)}, u32[]{:S(2)}) %collective-permute-start.2) | collective-permute-done | bytes 786464 | tf_op jit(solution)/shard_map/ppermute | solution.py:47
  52.1 7.2 %fusion.14 = bf16[384,4096]{1,0:T(8,128)(2,1)} fusion(s32[]{:T(128)S(6)} %select_n.13, bf16[384,1024]{1,0:T(8,128)(2,1)} %collective-permute-done.2, bf16[384,1024]{1,0:T(8,128)(2,1)S(1)} %collective-permute-done.1, bf16[384,1024]{1,0:T(8,128)(2,1)S(1)} %collective-permute-done, bf16[384,1024]{1,0:T(8,128)(2,1)S(1)} %fusion.20), kind=kLoop, calls=%fused_computation.38 | loop fusion | flops 25165824 | bytes 6291460 | tf_op jit(solution)/shard_map/jit(_roll_dynamic)/concatenate | solution.py:48
  59.3 102.0 %all-gather.6.cloned.1.call-done = bf16[2,4096,512]{2,1,0:T(8,128)(2,1)} async-done(((bf16[2,1024,512]{2,1,0:T(8,128)(2,1)}), bf16[2,4096,512]{2,1,0:T(8,128)(2,1)}) %all-gather.6.cloned.1.call-update) | async-done | bytes 8388624 | tf_op jit(solution)/shard_map/all_gather | solution.py:35
  161.3 5.0 fusion.37
  166.4 144.3 %all-gather.4.cloned.1.call-done = bf16[2,4096,512]{2,1,0:T(8,128)(2,1)} async-done(((bf16[2,1024,512]{2,1,0:T(8,128)(2,1)}), bf16[2,4096,512]{2,1,0:T(8,128)(2,1)}) %all-gather.4.cloned.1.call-update) | async-done | bytes 8388624 | tf_op jit(solution)/shard_map/all_gather | solution.py:34
  310.7 4.9 fusion.39
  315.6 1.3 collective-permute-start.3
  317.0 1.6 collective-permute-done.3
  319.0 1.9 fusion.79
  322.2 6.6 %all-reduce.1 = (f32[384]{0:T(512)S(1)}, f32[384]{0:T(512)S(1)}) all-reduce(f32[384]{0:T(512)S(1)} %get-tuple-element.24, f32[384]{0:T(512)S(1)} %get-tuple-element.25), channel_id=1, replica_groups=mesh['grp'=2,'sp'=4,'tp'=4] {'tp'}, use_global_device_ids=true, to_apply=%region_5.7 | all-reduce | flops 768 | bytes 6144 | tf_op jit(solution)/shard_map/psum | solution.py:60
  328.8 131.3 %all-gather.8.cloned.1.call-done = bf16[2,512,4096]{2,1,0:T(8,128)(2,1)} async-done(((bf16[2,512,1024]{2,1,0:T(8,128)(2,1)}), bf16[2,512,4096]{2,1,0:T(8,128)(2,1)}) %all-gather.8.cloned.1.call-update) | async-done | bytes 8388624 | tf_op jit(solution)/shard_map/all_gather | solution.py:37
  460.1 5.9 convolution_convert_fusion.1
  466.2 35.8 %reduce-scatter.3.cloned.1.call-done = bf16[384,1024]{1,0:T(8,128)(2,1)} async-done(((bf16[384,4096]{1,0:T(8,128)(2,1)}), bf16[384,1024]{1,0:T(8,128)(2,1)}) %reduce-scatter.3.cloned.1.call-update) | async-done | bytes 786448 | tf_op jit(solution)/shard_map/reduce_scatter | solution.py:70
  502.0 1.5 fusion.22
  503.5 5.8 psum.45
  509.3 1.4 fusion.24
  510.8 11.4 %collective-permute-done.4 = bf16[384,1024]{1,0:T(8,128)(2,1)S(1)} collective-permute-done((bf16[384,1024]{1,0:T(8,128)(2,1)S(1)}, bf16[384,1024]{1,0:T(8,128)(2,1)S(1)}, u32[]{:S(2)}, u32[]{:S(2)}) %collective-permute-start.4) | collective-permute-done | bytes 786464 | tf_op jit(solution)/shard_map/ppermute | solution.py:47
  522.2 11.4 %collective-permute-done.5 = bf16[384,1024]{1,0:T(8,128)(2,1)S(1)} collective-permute-done((bf16[384,1024]{1,0:T(8,128)(2,1)S(1)}, bf16[384,1024]{1,0:T(8,128)(2,1)S(1)}, u32[]{:S(2)}, u32[]{:S(2)}) %collective-permute-start.5) | collective-permute-done | bytes 786464 | tf_op jit(solution)/shard_map/ppermute | solution.py:47
  533.6 11.4 %collective-permute-done.6 = bf16[384,1024]{1,0:T(8,128)(2,1)S(1)} collective-permute-done((bf16[384,1024]{1,0:T(8,128)(2,1)S(1)}, bf16[384,1024]{1,0:T(8,128)(2,1)S(1)}, u32[]{:S(2)}, u32[]{:S(2)}) %collective-permute-start.6) | collective-permute-done | bytes 786464 | tf_op jit(solution)/shard_map/ppermute | solution.py:47
  545.0 5.4 fusion.7
  550.4 4.3 fusion.35
  554.7 1.8 fusion.38
  556.5 3.6 collective-permute-start.7
  560.1 1.6 collective-permute-done.7
  562.2 2.0 fusion.80
  565.7 5.7 all-reduce
  571.4 6.0 convolution_convert_fusion
  577.3 39.2 %reduce-scatter.5.cloned.1.call-done = bf16[384,1024]{1,0:T(8,128)(2,1)} async-done(((bf16[384,4096]{1,0:T(8,128)(2,1)}), bf16[384,1024]{1,0:T(8,128)(2,1)}) %reduce-scatter.5.cloned.1.call-update) | async-done | bytes 786448 | tf_op jit(solution)/shard_map/reduce_scatter | solution.py:70
  616.5 2.4 fusion.25
  (69 shorter events, 6.8 us)
Async XLA Ops:
  6.5 2.3 copy-start
  6.5 10.9 %copy-start.2 = (f32[2,1024]{1,0:T(2,128)S(1)}, f32[2,1024]{1,0:T(2,128)}, u32[]{:S(2)}) copy-start(f32[2,1024]{1,0:T(2,128)} %param.11) | copy-start | bytes 24580
  6.5 34.0 %copy-start.3 = (f32[2,512]{1,0:T(2,128)S(1)}, f32[2,512]{1,0:T(2,128)}, u32[]{:S(2)}) copy-start(f32[2,512]{1,0:T(2,128)} %param.15) | copy-start | bytes 12292
  6.5 154.7 %all-gather.6.cloned.1.call-start = ((), (), s32[]{:S(2)}) async-start(), calls=%async_computation.3 | async-start | bytes 10485760 | tf_op jit(solution)/shard_map/all_gather | solution.py:35
  7.3 303.4 %all-gather.4.cloned.1.call-start = ((), (), s32[]{:S(2)}) async-start(), calls=%async_computation.2 | async-start | bytes 10485760 | tf_op jit(solution)/shard_map/all_gather | solution.py:34
  8.0 452.1 %all-gather.8.cloned.1.call-start = ((), (), s32[]{:S(2)}) async-start(), calls=%async_computation.4 | async-start | bytes 10485760 | tf_op jit(solution)/shard_map/all_gather | solution.py:37
  8.7 493.3 %reduce-scatter.3.cloned.1.call-start = ((), (), s32[]{:S(2)}) async-start(), calls=%async_computation.5 | async-start | bytes 3932160 | tf_op jit(solution)/shard_map/reduce_scatter | solution.py:70
  17.7 11.5 %collective-permute-start = (bf16[384,1024]{1,0:T(8,128)(2,1)S(1)}, bf16[384,1024]{1,0:T(8,128)(2,1)S(1)}, u32[]{:S(2)}, u32[]{:S(2)}) collective-permute-start(bf16[384,1024]{1,0:T(8,128)(2,1)S(1)} %fusion.20), channel_id=1, source_target_pairs={{0,1},{1,2},{2,3},{3,0},{4,5},{5,6},{6,7},{7,4},{8,9},{9,10},{10,1... | collective-permute-start | bytes 2359304 | tf_op jit(solution)/shard_map/ppermute | solution.py:47
  29.1 11.4 %collective-permute-start.1 = (bf16[384,1024]{1,0:T(8,128)(2,1)S(1)}, bf16[384,1024]{1,0:T(8,128)(2,1)S(1)}, u32[]{:S(2)}, u32[]{:S(2)}) collective-permute-start(bf16[384,1024]{1,0:T(8,128)(2,1)S(1)} %collective-permute-done), channel_id=1, source_target_pairs={{0,1},{1,2},{2,3},{3,0},{4,5},{5,6},{6,7},{7,4},{8,9},{9,10},{10,1... | collective-permute-start | bytes 2359304 | tf_op jit(solution)/shard_map/ppermute | solution.py:47
  40.6 11.5 %collective-permute-start.2 = (bf16[384,1024]{1,0:T(8,128)(2,1)S(1)}, bf16[384,1024]{1,0:T(8,128)(2,1)}, u32[]{:S(2)}, u32[]{:S(2)}) collective-permute-start(bf16[384,1024]{1,0:T(8,128)(2,1)S(1)} %collective-permute-done.1), channel_id=1, source_target_pairs={{0,1},{1,2},{2,3},{3,0},{4,5},{5,6},{6,7},{7,4},{8,9},{9,10},{10,1... | collective-permute-start | bytes 2359304 | tf_op jit(solution)/shard_map/ppermute | solution.py:47
  166.3 150.6 %copy-start.4 = (f32[2,512]{1,0:T(2,128)S(1)}, f32[2,512]{1,0:T(2,128)}, u32[]{:S(2)}) copy-start(f32[2,512]{1,0:T(2,128)} %param.16) | copy-start | bytes 12292
  166.3 152.6 %copy-start.5 = (f32[2,31,512]{2,0,1:T(2,128)S(1)}, f32[2,31,512]{2,0,1:T(2,128)}, u32[]{:S(2)}) copy-start(f32[2,31,512]{2,0,1:T(2,128)} %param.14) | copy-start | bytes 380932
  166.3 152.6 %copy-start.6 = (pred[8,52]{0,1:T(8,128)(4,1)S(1)}, pred[8,52]{0,1:T(8,128)(4,1)}, u32[]{:S(2)}) copy-start(pred[8,52]{0,1:T(8,128)(4,1)} %constant.56) | copy-start | bytes 1252
  315.6 2.9 collective-permute-start.3
  466.0 150.5 %reduce-scatter.5.cloned.1.call-start = ((), (), s32[]{:S(2)}) async-start(), calls=%async_computation.6 | async-start | bytes 3932160 | tf_op jit(solution)/shard_map/reduce_scatter | solution.py:70
  510.7 11.5 %collective-permute-start.4 = (bf16[384,1024]{1,0:T(8,128)(2,1)S(1)}, bf16[384,1024]{1,0:T(8,128)(2,1)S(1)}, u32[]{:S(2)}, u32[]{:S(2)}) collective-permute-start(bf16[384,1024]{1,0:T(8,128)(2,1)S(1)} %fusion.24), channel_id=1, source_target_pairs={{0,1},{1,2},{2,3},{3,0},{4,5},{5,6},{6,7},{7,4},{8,9},{9,10},{10,1... | collective-permute-start | bytes 2359304 | tf_op jit(solution)/shard_map/ppermute | solution.py:47
  522.2 11.4 %collective-permute-start.5 = (bf16[384,1024]{1,0:T(8,128)(2,1)S(1)}, bf16[384,1024]{1,0:T(8,128)(2,1)S(1)}, u32[]{:S(2)}, u32[]{:S(2)}) collective-permute-start(bf16[384,1024]{1,0:T(8,128)(2,1)S(1)} %collective-permute-done.4), channel_id=1, source_target_pairs={{0,1},{1,2},{2,3},{3,0},{4,5},{5,6},{6,7},{7,4},{8,9},{9,10},{10,1... | collective-permute-start | bytes 2359304 | tf_op jit(solution)/shard_map/ppermute | solution.py:47
  533.6 11.4 %collective-permute-start.6 = (bf16[384,1024]{1,0:T(8,128)(2,1)S(1)}, bf16[384,1024]{1,0:T(8,128)(2,1)S(1)}, u32[]{:S(2)}, u32[]{:S(2)}) collective-permute-start(bf16[384,1024]{1,0:T(8,128)(2,1)S(1)} %collective-permute-done.5), channel_id=1, source_target_pairs={{0,1},{1,2},{2,3},{3,0},{4,5},{5,6},{6,7},{7,4},{8,9},{9,10},{10,1... | collective-permute-start | bytes 2359304 | tf_op jit(solution)/shard_map/ppermute | solution.py:47
  545.0 9.7 %slice-start = ((s8[8388608]{0:T(1024)(128)(4,1)}), s8[4194304]{0:T(1024)(128)(4,1)S(1)}, s32[]{:S(2)}) async-start(s8[8388608]{0:T(1024)(128)(4,1)} %bitcast.88), calls=%async_computation.7 | async-start | bytes 8388608
  550.4 4.3 slice-start.1
  554.7 7.4 %copy-start.7 = (pred[8,52]{0,1:T(8,128)(4,1)S(1)}, pred[8,52]{0,1:T(8,128)(4,1)}, u32[]{:S(2)}) copy-start(pred[8,52]{0,1:T(8,128)(4,1)} %constant.56) | copy-start | bytes 1252
  556.5 5.2 collective-permute-start.7
  571.3 45.2 %copy-start.1 = (bf16[384,1024]{1,0:T(8,128)(2,1)S(1)}, bf16[384,1024]{1,0:T(8,128)(2,1)}, u32[]{:S(2)}) copy-start(bf16[384,1024]{1,0:T(8,128)(2,1)} %reduce-scatter.3.cloned.1.call-done) | copy-start | bytes 2359300
Sparse Core Ops, SparseCore 0:
  8.9 152.3 all-gather.5
  162.8 147.7 all-gather.3
  312.3 147.7 all-gather.7
  466.1 35.8 reduce-scatter.2
  577.5 38.9 reduce-scatter.4
